TPU v7x, 256 devices: a whole 4x4x8 slice. The times are simulated.
256 devices in a mesh: ep: 64 (over z, x, core), tp: 4 (over y).
Axes of the slice: x: 4, y: 4, z: 8, core: 2. Of those that a mesh axis runs over, the one named last changes fastest.
Arguments:
- out_gate: bfloat16 [32768, 2048], P(('ep', 'tp')), may hold values from -6 to 6
- in_gate: bfloat16 [32768, 2048], P(('ep', 'tp')), may hold values from -6 to 6
- conv_input: bfloat16 [32768, 2048], P(('ep', 'tp')), may hold values from -6 to 6
- conv_taps: bfloat16 [3, 2048], replicated, may hold values from -3 to 3
- mixer_weight: bfloat16 [2048, 2048], P(None, 'tp'), may hold values from -0.125 to 0.125
- expert_input: bfloat16 [32768, 2048], P(('ep', 'tp')), may hold values from -6 to 6
- norm_gain: float32 [2048], replicated, may hold values from 0.1 to 1.9
- expert_gate: bfloat16 [64, 2048, 1024], P('ep', None, 'tp'), may hold values from -0.125 to 0.125
- expert_up: bfloat16 [64, 2048, 1024], P('ep', None, 'tp'), may hold values from -0.125 to 0.125
- expert_down: bfloat16 [64, 1024, 2048], P('ep', 'tp'), may hold values from -0.1875 to 0.1875
- expert_ids: int32 [32768, 2], P(('ep', 'tp')), may hold values from 0 to 63, all different within a row; in each aligned block of 128 rows (0 to 127, 128 to 255, ...) at most 8 rows name the same one
- route_weight: float32 [32768, 2], P(('ep', 'tp')), may hold values from 0.1 to 1
Outputs:
- mixer_out: bfloat16 [32768, 2048], P('ep', 'tp')
- experts_out: bfloat16 [32768, 2048], P(('ep', 'tp'))
Inputs may be any that keep to these rules, and one draw needn't show every extreme that they name: `expert_ids`: each row names 2 different experts. Within the 128 rows of one device no expert is named by more than 8 rows, and in some devices' rows some expert is named by exactly 8.
All inputs are finite; a program needn't handle non-finite values.
Results may differ from a plain program's by a relative error of at most 0.011.
Values may be sent and summed in bfloat16 or wider, within the bound.
No kernel may reach another device: no remote copies, remote signals or barrier semaphores. Data moves between devices by JAX's collectives and lax.ppermute only.
A program may use at most 128 MiB of HBM per device.

v0:
```python
import jax
import jax.numpy as jnp
from jax import lax
from jax.sharding import PartitionSpec as P

CONV = 3
SEQS = 1
norm_eps = 1e-06


def from_behind(value, axis, steps):
    count = lax.axis_size(axis)
    first, last = (max(0, -steps), min(count, count - steps))
    return lax.ppermute(value, axis, [(source, source + steps) for source in range(first, last)])


def turned_gather(arrays, axis, dims):
    turned = [jnp.moveaxis(a, dim, 0) for a, dim in zip(arrays, dims)]
    both = jnp.concatenate([t.reshape(len(t), -1) for t in turned], axis=1)
    whole, at, done = (lax.all_gather(both, axis, axis=0, tiled=True), 0, [])
    for t, dim in zip(turned, dims):
        piece = whole[:, at : at + t[0].size].reshape(-1, *t.shape[1:])
        done.append(jnp.moveaxis(piece, 0, dim))
        at += t[0].size
    return tuple(done)


def sent_to_all(x, axis):
    count = lax.axis_size(axis)
    return lax.all_to_all(jnp.broadcast_to(x[None], (count, *x.shape)), axis, 0, 0, tiled=True)


def joined_along(tiles, dim):
    dims = list(tiles.shape[1:])
    dims[dim] *= tiles.shape[0]
    return jnp.moveaxis(tiles, 0, dim).reshape(dims)


def gathered_copies(x, axis, dim):
    tiles = sent_to_all(x, axis)
    return joined_along(tiles, dim)


def device_slots(route_ids, expert_count):
    flat_ids = route_ids.reshape(-1)
    member = (flat_ids[:, None] == jnp.arange(expert_count, dtype=jnp.int32)[None, :]).astype(
        jnp.int32
    )
    before = jnp.cumsum(member, axis=0) - member
    return jnp.sum(before * member, axis=1).reshape(route_ids.shape)


def fill_slots(row_data, route_ids, expert_count, slot_cap):
    top_count = route_ids.shape[1]
    position = (route_ids * slot_cap + device_slots(route_ids, expert_count)).reshape(-1)
    zeroed = jnp.zeros((expert_count * slot_cap, row_data.shape[1]), row_data.dtype)
    return zeroed.at[position].set(jnp.repeat(row_data, top_count, axis=0))


def expert_hidden(slot_rows, w_gate, w_up):
    gate_proj = jnp.dot(slot_rows, w_gate, preferred_element_type=jnp.float32)
    up_proj = jnp.dot(slot_rows, w_up, preferred_element_type=jnp.float32)
    return (jax.nn.silu(gate_proj) * up_proj).astype(jnp.bfloat16)


def local(
    out_gate,
    in_gate,
    conv_input,
    conv_taps,
    mixer_weight,
    expert_input,
    norm_gain,
    expert_gate,
    expert_up,
    expert_down,
    expert_ids,
    route_weight,
):
    row_count = in_gate.shape[0]
    tap_span = CONV - 1
    group_size = lax.axis_size("tp")
    product = in_gate.astype(jnp.float32) * conv_input.astype(jnp.float32)
    edge_product = from_behind(product[row_count - tap_span :], ("ep", "tp"), 1)
    seq_length = row_count * lax.axis_size("ep") * group_size // SEQS
    linear_index = lax.axis_index("ep") * group_size + lax.axis_index("tp")
    carry_over = jnp.where(linear_index * row_count % seq_length == 0, 0.0, 1.0).astype(jnp.float32)
    earlier = edge_product * carry_over
    padded = jnp.concatenate([earlier, product], axis=0)
    tap_values = conv_taps.astype(jnp.float32)
    smoothed = sum(
        (
            padded[tap_index : tap_index + row_count] * tap_values[tap_index]
            for tap_index in range(CONV)
        )
    )
    gated = (out_gate.astype(jnp.float32) * smoothed).astype(jnp.bfloat16)
    token_count = expert_input.shape[0]
    model_width = expert_input.shape[1]
    expert_count = lax.axis_size("ep")
    slot_cap = 4 * token_count // expert_count
    wide_input = expert_input.astype(jnp.float32)
    inv_norm = lax.rsqrt(jnp.mean(wide_input * wide_input, axis=1, keepdims=True) + norm_eps)
    normed = (wide_input * inv_norm * norm_gain).astype(jnp.bfloat16)
    w_gate = expert_gate[0]
    hidden_width = w_gate.shape[1]
    position = (expert_ids * slot_cap + device_slots(expert_ids, expert_count)).reshape(-1)
    whole_gate, whole_up, whole_down = turned_gather(
        (expert_gate, expert_up, expert_down), "tp", (2, 2, 1)
    )
    mixer_out = jnp.dot(
        gathered_copies(gated, "tp", 0), mixer_weight, preferred_element_type=jnp.float32
    ).astype(jnp.bfloat16)
    outgoing = fill_slots(normed, expert_ids, expert_count, slot_cap).reshape(
        expert_count, slot_cap, model_width
    )
    arrived = lax.all_to_all(outgoing, "ep", split_axis=0, concat_axis=0, tiled=True)
    hidden = expert_hidden(arrived.reshape(-1, model_width), whole_gate[0], whole_up[0])
    running = jnp.zeros((hidden.shape[0], model_width), jnp.float32)
    for quarter in range(group_size):
        partial_sum = jnp.dot(
            hidden[:, quarter * hidden_width : (quarter + 1) * hidden_width],
            whole_down[0, quarter * hidden_width : (quarter + 1) * hidden_width],
            preferred_element_type=jnp.float32,
        )
        running = running + lax.optimization_barrier(partial_sum.astype(jnp.bfloat16)).astype(
            jnp.float32
        )
    summed = running.astype(jnp.bfloat16)
    returned = lax.all_to_all(
        summed.reshape(expert_count, slot_cap, model_width),
        "ep",
        split_axis=0,
        concat_axis=0,
        tiled=True,
    )
    picked = returned.reshape(expert_count * slot_cap, model_width)[position]
    top_count = expert_ids.shape[1]
    picked = picked.reshape(token_count, top_count, model_width).astype(jnp.float32)
    route_share = route_weight / jnp.sum(route_weight, axis=1, keepdims=True)
    experts_out = jnp.sum(picked * route_share[:, :, None], axis=1).astype(jnp.bfloat16)
    return (mixer_out, experts_out)


def solution(mesh):
    return jax.shard_map(
        local,
        mesh=mesh,
        in_specs=(
            P(("ep", "tp"), None),
            P(("ep", "tp"), None),
            P(("ep", "tp"), None),
            P(),
            P(None, "tp"),
            P(("ep", "tp"), None),
            P(),
            P("ep", None, "tp"),
            P("ep", None, "tp"),
            P("ep", "tp", None),
            P(("ep", "tp"), None),
            P(("ep", "tp"), None),
        ),
        out_specs=(P("ep", "tp"), P(("ep", "tp"), None)),
        check_vma=False,
    )
```

profile of v0, /device:TPU:2, one launch (start us, length us, event | category | flops | bytes accessed | tf_op | source)
XLA Modules:
  0.0 256.6 jit_solution(5777766313457616433)
XLA Ops:
  7.2 0.0 copy-start
  7.2 0.0 all-gather.2.cloned.1.call-start
  7.2 1.6 copy.31
  8.9 2.3 copy.30
  11.1 3.0 %pad_maximum_fusion = bf16[256,6144]{1,0:T(8,128)(2,1)} fusion(bf16[256,2048]{1,0:T(8,128)(2,1)} %bitcast.77, bf16[256,2048]{1,0:T(8,128)(2,1)S(1)} %bitcast.75, bf16[256,2048]{1,0:T(8,128)(2,1)} %bitcast.76), kind=kLoop, calls=%fused_computation.8 | loop fusion | flops 9437184 | bytes 6291456 | tf_op jit(solution)/shard_map/concatenate | solution.py:19
  14.1 0.0 copy-start.6
  14.1 0.0 copy-start.2
  14.1 0.0 copy-start.5
  14.2 0.0 all-gather.2.cloned.1.call-update
  14.2 0.6 copy-done.6
  14.8 0.1 copy.25
  14.9 0.1 eq.42
  15.1 0.1 eq.38
  15.2 0.6 reduce-window.6
  15.8 0.2 slice_reduce_fusion
  16.1 0.1 fusion.25
  16.2 0.1 reshape.104
  16.3 0.1 copy.28
  16.4 0.1 copy.29
  16.5 0.1 reshape.105
  16.7 0.0 copy-done.2
  16.7 0.2 fusion.13
  16.9 0.0 copy-done.5
  16.9 0.2 fusion.15
  17.1 0.6 broadcast_in_dim.8
  17.7 1.2 reshape.128
  19.0 4.4 %scatter_custom_fusion = bf16[512,2048]{1,0:T(8,128)(2,1)} fusion(s32[256]{0:T(256)S(1)} %bitcast.81, bf16[256,2048]{1,0:T(8,128)(2,1)} %reshape.128, bf16[]{:T(256)} %constant.45.clone.1), kind=kCustom, calls=%fused_computation.38 | custom fusion | bytes 2097664 | tf_op jit(solution)/shard_map/scatter | solution.py:57
  23.4 12.2 %all-to-all-start.1 = ((bf16[64,8,2048]{2,1,0:T(8,128)(2,1)}), bf16[64,8,2048]{2,1,0:T(8,128)(2,1)}, u32[]{:S(2)}, u32[]{:S(2)}) async-start(bf16[64,8,2048]{2,1,0:T(8,128)(2,1)} %bitcast.74), calls=%async_computation.1 | async-start | bytes 4194304 | tf_op jit(solution)/shard_map/all_to_all | solution.py:117
  35.6 0.0 copy-start.4
  35.6 1.4 convert_multiply_fusion.2
  37.1 3.5 %collective-permute-start = (f32[2,2048]{1,0:T(2,128)S(1)}, f32[2,2048]{1,0:T(2,128)S(1)}, u32[]{:S(2)}, u32[]{:S(2)}) collective-permute-start(f32[2,2048]{1,0:T(2,128)S(1)} %slice.78), channel_id=1, source_target_pairs={{0,1},{1,2},{2,3},{3,4},{4,5},{5,6},{6,7},{7,8},{8,9},{9,10},{10,1... | collective-permute-start | bytes 49160 | tf_op jit(solution)/shard_map/ppermute | solution.py:14
  40.6 0.0 copy-done.4
  40.6 3.7 %collective-permute-done = f32[2,2048]{1,0:T(2,128)S(1)} collective-permute-done((f32[2,2048]{1,0:T(2,128)S(1)}, f32[2,2048]{1,0:T(2,128)S(1)}, u32[]{:S(2)}, u32[]{:S(2)}) %collective-permute-start) | collective-permute-done | bytes 16416 | tf_op jit(solution)/shard_map/ppermute | solution.py:14
  44.4 2.2 fusion.12
  46.6 0.0 copy-start.3
  46.6 91.8 %all-gather.2.cloned.1.call-done = bf16[1024,6144]{1,0:T(8,128)(2,1)} async-done(((bf16[256,6144]{1,0:T(8,128)(2,1)}), bf16[1024,6144]{1,0:T(8,128)(2,1)}) %all-gather.2.cloned.1.call-update) | async-done | bytes 12582928 | tf_op jit(solution)/shard_map/all_gather | solution.py:20
  138.4 4.7 %slice_bitcast_fusion = bf16[1,1024,2048]{2,1,0:T(8,128)(2,1)} fusion(bf16[1024,6144]{1,0:T(8,128)(2,1)} %all-gather.2.cloned.1.call-done), kind=kLoop, calls=%fused_computation.2 | loop fusion | bytes 8388608 | tf_op jit(solution)/shard_map/transpose;reshape | solution.py:23
  143.1 0.0 all-to-all-done.1
  143.1 0.0 copy-done.3
  143.1 1.6 broadcast_in_dim.6
  144.7 4.6 %all-to-all-start = ((bf16[4,128,2048]{2,1,0:T(8,128)(2,1)}), bf16[4,128,2048]{2,1,0:T(8,128)(2,1)}, u32[]{:S(2)}, u32[]{:S(2)}) async-start(bf16[4,128,2048]{2,1,0:T(8,128)(2,1)} %broadcast_in_dim.6), calls=%async_computation | async-start | bytes 4194304 | tf_op jit(solution)/shard_map/all_to_all | solution.py:30
  149.4 5.2 %fusion.1 = f32[512,1024]{1,0:T(8,128)S(1)} fusion(bf16[1024,6144]{1,0:T(8,128)(2,1)} %all-gather.2.cloned.1.call-done, bf16[64,8,2048]{2,1,0:T(8,128)(2,1)} %all-to-all-done.1), kind=kOutput, calls=%fused_computation.6 | convolution fusion | flops 2147483648 | bytes 8388608 | tf_op jit(solution)/shard_map/dot_general | solution.py:61
  154.5 0.0 copy-start.1
  154.6 5.5 %multiply_convert_fusion = bf16[512,1024]{1,0:T(8,128)(2,1)S(1)} fusion(f32[512,1024]{1,0:T(8,128)S(1)} %fusion.1, bf16[1024,6144]{1,0:T(8,128)(2,1)} %all-gather.2.cloned.1.call-done, bf16[64,8,2048]{2,1,0:T(8,128)(2,1)} %all-to-all-done.1), kind=kOutput, calls=%fused_computation.17 | convolution fusion | flops 2150629376 | bytes 9437184 | tf_op jit(solution)/shard_map/dot_general | solution.py:62
  160.1 0.0 copy-done.1
  160.1 0.7 convolution_convert_fusion.3
  160.8 0.7 convolution_convert_fusion.2
  161.5 0.7 convolution_convert_fusion.1
  162.2 0.7 convolution_convert_fusion
  163.0 3.1 %fusion.2 = bf16[64,8,2048]{2,1,0:T(8,128)(2,1)} fusion(bf16[512,2048]{1,0:T(8,128)(2,1)S(1)} %convolution_convert_fusion, bf16[512,2048]{1,0:T(8,128)(2,1)S(1)} %convolution_convert_fusion.1, bf16[512,2048]{1,0:T(8,128)(2,1)S(1)} %convolution_convert_fusion.2, bf16[512,2048]{1,0:T(8,128)(2,1)S(1)} %convolution_convert_fusion.3), kind=kLoop, calls=%fused_computation.13 | loop fusion | flops 8388608 | bytes 10485760 | tf_op jit(solution)/shard_map/reshape | solution.py:131
  166.1 0.0 copy-start.7
  166.1 9.6 %all-to-all-done = bf16[4,128,2048]{2,1,0:T(8,128)(2,1)} async-done(((bf16[4,128,2048]{2,1,0:T(8,128)(2,1)}), bf16[4,128,2048]{2,1,0:T(8,128)(2,1)}, u32[]{:S(2)}, u32[]{:S(2)}) %all-to-all-start) | async-done | bytes 2097184 | tf_op jit(solution)/shard_map/all_to_all | solution.py:30
  175.7 10.7 %all-to-all-start.2 = ((bf16[64,8,2048]{2,1,0:T(8,128)(2,1)}), bf16[64,8,2048]{2,1,0:T(8,128)(2,1)}, u32[]{:S(2)}, u32[]{:S(2)}) async-start(bf16[64,8,2048]{2,1,0:T(8,128)(2,1)} %fusion.2), calls=%async_computation.2 | async-start | bytes 4194304 | tf_op jit(solution)/shard_map/all_to_all | solution.py:130
  186.4 0.0 copy-done.7
  186.5 0.1 copy.32
  186.6 0.0 copy-done
  186.6 3.6 %convolution_convert_fusion.4 = bf16[512,512]{1,0:T(8,128)(2,1)} fusion(bf16[512,2048]{1,0:T(8,128)(2,1)} %bitcast.3, bf16[2048,512]{1,0:T(8,128)(2,1)S(1)} %copy-done), kind=kOutput, calls=%fused_computation.20 | convolution fusion | flops 1074003968 | bytes 4718592 | tf_op jit(solution)/shard_map/dot_general | solution.py:111
  190.2 47.3 %all-to-all-done.2 = bf16[64,8,2048]{2,1,0:T(8,128)(2,1)} async-done(((bf16[64,8,2048]{2,1,0:T(8,128)(2,1)}), bf16[64,8,2048]{2,1,0:T(8,128)(2,1)}, u32[]{:S(2)}, u32[]{:S(2)}) %all-to-all-start.2) | async-done | bytes 2097184 | tf_op jit(solution)/shard_map/all_to_all | solution.py:130
  237.6 4.2 %gather_fusion = bf16[256,2048]{1,0:T(8,128)(2,1)S(1)} fusion(bf16[512,2048]{1,0:T(8,128)(2,1)} %bitcast.25, s32[1024]{0:T(1024)S(1)} %pad_clamp_fusion), kind=kCustom, calls=%fused_computation | custom fusion | bytes 2098176 | tf_op jit(solution)/shard_map/gather | solution.py:137
  241.8 2.4 reshape.115
  244.2 5.6 %multiply_reduce_fusion = bf16[128,2048]{1,0:T(8,128)(2,1)} fusion(f32[128,2,2048]{2,1,0:T(2,128)} %reshape.115, f32[128,2]{1,0:T(8,128)S(1)} %copy.32), kind=kLoop, calls=%fused_computation.16 | loop fusion | flops 786432 | bytes 2622464 | tf_op jit(solution)/shard_map/reduce_sum | solution.py:141
  (12 shorter events, 0.1 us)
Async XLA Ops:
  7.2 179.4 %copy-start = (bf16[2048,512]{1,0:T(8,128)(2,1)S(1)}, bf16[2048,512]{1,0:T(8,128)(2,1)}, u32[]{:S(2)}) copy-start(bf16[2048,512]{1,0:T(8,128)(2,1)} %param.16) | copy-start | bytes 6291460
  7.2 131.2 %all-gather.2.cloned.1.call-start = ((), (), s32[]{:S(2)}) async-start(), calls=%async_computation.3 | async-start | bytes 15728640 | tf_op jit(solution)/shard_map/all_gather | solution.py:20
  14.1 0.7 copy-start.6
  14.1 2.5 copy-start.2
  14.1 2.7 %copy-start.5 = (f32[2048]{0:T(1024)S(1)}, f32[2048]{0:T(1024)}, u32[]{:S(2)}) copy-start(f32[2048]{0:T(1024)} %param.18) | copy-start | bytes 24580
  23.4 119.7 %all-to-all-start.1 = ((bf16[64,8,2048]{2,1,0:T(8,128)(2,1)}), bf16[64,8,2048]{2,1,0:T(8,128)(2,1)}, u32[]{:S(2)}, u32[]{:S(2)}) async-start(bf16[64,8,2048]{2,1,0:T(8,128)(2,1)} %bitcast.74), calls=%async_computation.1 | async-start | bytes 4194304 | tf_op jit(solution)/shard_map/all_to_all | solution.py:117
  35.6 5.0 %copy-start.4 = (bf16[3,2048]{1,0:T(4,128)(2,1)S(1)}, bf16[3,2048]{1,0:T(4,128)(2,1)}, u32[]{:S(2)}) copy-start(bf16[3,2048]{1,0:T(4,128)(2,1)} %param.15) | copy-start | bytes 36868
  37.1 7.3 %collective-permute-start = (f32[2,2048]{1,0:T(2,128)S(1)}, f32[2,2048]{1,0:T(2,128)S(1)}, u32[]{:S(2)}, u32[]{:S(2)}) collective-permute-start(f32[2,2048]{1,0:T(2,128)S(1)} %slice.78), channel_id=1, source_target_pairs={{0,1},{1,2},{2,3},{3,4},{4,5},{5,6},{6,7},{7,8},{8,9},{9,10},{10,1... | collective-permute-start | bytes 49160 | tf_op jit(solution)/shard_map/ppermute | solution.py:14
  46.6 96.5 %copy-start.3 = (bf16[128,2048]{1,0:T(8,128)(2,1)S(1)}, bf16[128,2048]{1,0:T(8,128)(2,1)}, u32[]{:S(2)}) copy-start(bf16[128,2048]{1,0:T(8,128)(2,1)} %fusion.12) | copy-start | bytes 1572868
  144.7 31.0 %all-to-all-start = ((bf16[4,128,2048]{2,1,0:T(8,128)(2,1)}), bf16[4,128,2048]{2,1,0:T(8,128)(2,1)}, u32[]{:S(2)}, u32[]{:S(2)}) async-start(bf16[4,128,2048]{2,1,0:T(8,128)(2,1)} %broadcast_in_dim.6), calls=%async_computation | async-start | bytes 4194304 | tf_op jit(solution)/shard_map/all_to_all | solution.py:30
  154.5 5.5 %copy-start.1 = (bf16[1,1024,2048]{2,1,0:T(8,128)(2,1)S(1)}, bf16[1,1024,2048]{2,1,0:T(8,128)(2,1)}, u32[]{:S(2)}) copy-start(bf16[1,1024,2048]{2,1,0:T(8,128)(2,1)} %slice_bitcast_fusion) | copy-start | bytes 12582916
  166.1 20.3 %copy-start.7 = (f32[128,2]{0,1:T(2,128)S(1)}, f32[128,2]{0,1:T(2,128)}, u32[]{:S(2)}) copy-start(f32[128,2]{0,1:T(2,128)} %param.23) | copy-start | bytes 3076
  175.7 61.9 %all-to-all-start.2 = ((bf16[64,8,2048]{2,1,0:T(8,128)(2,1)}), bf16[64,8,2048]{2,1,0:T(8,128)(2,1)}, u32[]{:S(2)}, u32[]{:S(2)}) async-start(bf16[64,8,2048]{2,1,0:T(8,128)(2,1)} %fusion.2), calls=%async_computation.2 | async-start | bytes 4194304 | tf_op jit(solution)/shard_map/all_to_all | solution.py:130
Sparse Core Ops, SparseCore 0:
  14.3 124.0 all-gather.1
where the time goes:
time: 257 us
  waiting for transfers between devices  152 us (59%)
  starting transfers between devices  31.1 us (12%)
  local copies, waits for them, and re-layouts  25 us (10%)
  matrix products  17.2 us (7%)
  other arithmetic  16.6 us (6%)
  between operations  14.3 us (6%)
    all_gather x1, waiting for transfers between devices, turned_gather(): whole, at, done = (lax.all_gather(both, axis, axis=0, tiled=True), 0, [])  91.8 us
    all_to_all x1, waiting for transfers between devices, local(): lax.all_to_all(summed.reshape(expert_count, slot_cap, model_width), 'ep',...  47.3 us
    all_to_all x1, starting transfers between devices, local(): lax.all_to_all(outgoing, 'ep', split_axis=0, concat_axis=0, tiled=True)  12.2 us
    all_to_all x1, starting transfers between devices, local(): lax.all_to_all(summed.reshape(expert_count, slot_cap, model_width), 'ep',...  10.7 us
    all_to_all x1, waiting for transfers between devices, sent_to_all(): lax.all_to_all(jnp.broadcast_to(x[None], (count, *x.shape)), axis, 0, 0,...  9.56 us
    reduce_sum x1, other arithmetic, local(): jnp.sum(picked * route_share[:, :, None], axis=1).astype(jnp.bfloat16)  5.59 us
    dot_general x1, matrix products, expert_hidden(): up_proj = jnp.dot(slot_rows, w_up, preferred_element_type=jnp.float32)  5.5 us
    dot_general x1, matrix products, expert_hidden(): gate_proj = jnp.dot(slot_rows, w_gate, preferred_element_type=jnp.float32)  5.18 us
  transfers between devices with their start and end apart: 5, of which 4 were waited for; matrix products, arithmetic and copies ran while one was open for 15% of the time, Pallas kernels for 0%

commit v1 on v0

--- a/solution.py
+++ b/solution.py
@@ -6,6 +6,11 @@
 CONV = 3
 SEQS = 1
 norm_eps = 1e-06
+
+
+def all_by_exchange(array, name, along):
+    stack = jnp.stack([array] * lax.axis_size(name))
+    return jnp.concatenate(lax.all_to_all(stack, name, 0, 0), axis=along)
 
 
 def from_behind(value, axis, steps):
@@ -17,7 +22,7 @@
 def turned_gather(arrays, axis, dims):
     turned = [jnp.moveaxis(a, dim, 0) for a, dim in zip(arrays, dims)]
     both = jnp.concatenate([t.reshape(len(t), -1) for t in turned], axis=1)
-    whole, at, done = (lax.all_gather(both, axis, axis=0, tiled=True), 0, [])
+    whole, at, done = (all_by_exchange(both, axis, 0), 0, [])
     for t, dim in zip(turned, dims):
         piece = whole[:, at : at + t[0].size].reshape(-1, *t.shape[1:])
         done.append(jnp.moveaxis(piece, 0, dim))

time: 257 us -> 327 us (1.27)
  waiting for transfers between devices: 152 us -> 226 us
  between operations: 14.3 us -> 0.92 us
  local copies, waits for them, and re-layouts: 25 us -> 32.4 us
    all_to_all x0 -> x1, waiting for transfers between devices: none -> 130 us  [all_by_exchange(): return jnp.concatenate(lax.all_to_all(stack, name, 0, 0), axis=along)]
    all_gather x1 -> x0, waiting for transfers between devices: 91.8 us -> none  [turned_gather(): whole, at, done = (lax.all_gather(both, axis, axis=0, tiled=True), 0, [])]
    all_to_all x1, waiting for transfers between devices: 0.01 us -> 35.4 us  [local(): lax.all_to_all(outgoing, 'ep', split_axis=0, concat_axis=0, tiled=True)]
    another operation x1 -> x2, local copies, waits for them, and re-layouts: 0.01 us -> 7.95 us  [the longest x1 7.94 us: all_by_exchange(): stack = jnp.stack([array] * lax.axis_size(name))]
    all_to_all x0 -> x1, starting transfers between devices: none -> 6.46 us  [all_by_exchange(): return jnp.concatenate(lax.all_to_all(stack, name, 0, 0), axis=along)]
  transfers between devices with their start and end apart: 5 -> 5, of which waited for: 4 -> 5; matrix products, arithmetic and copies ran while one was open for 15% -> 11% of each run, Pallas kernels for 0% -> 0%
where the time goes in v1:
time: 327 us
  waiting for transfers between devices  226 us (69%)
  starting transfers between devices  33.4 us (10%)
  local copies, waits for them, and re-layouts  32.4 us (10%)
  matrix products  17.2 us (5%)
  other arithmetic  16.5 us (5%)
    all_to_all x1, waiting for transfers between devices, all_by_exchange(): return jnp.concatenate(lax.all_to_all(stack, name, 0, 0), axis=along)  130 us
    all_to_all x1, waiting for transfers between devices, local(): lax.all_to_all(summed.reshape(expert_count, slot_cap, model_width), 'ep',...  47.3 us
    all_to_all x1, waiting for transfers between devices, local(): lax.all_to_all(outgoing, 'ep', split_axis=0, concat_axis=0, tiled=True)  35.4 us
    all_to_all x1, starting transfers between devices, local(): lax.all_to_all(outgoing, 'ep', split_axis=0, concat_axis=0, tiled=True)  12.2 us
    all_to_all x1, waiting for transfers between devices, sent_to_all(): lax.all_to_all(jnp.broadcast_to(x[None], (count, *x.shape)), axis, 0, 0,...  8.19 us
    another operation x1, local copies, waits for them, and re-layouts, all_by_exchange(): stack = jnp.stack([array] * lax.axis_size(name))  7.94 us
    all_to_all x1, starting transfers between devices, local(): lax.all_to_all(summed.reshape(expert_count, slot_cap, model_width), 'ep',...  7.58 us
  transfers between devices with their start and end apart: 5, of which 5 were waited for; matrix products, arithmetic and copies ran while one was open for 11% of the time, Pallas kernels for 0%

profile of v1, /device:TPU:2, one launch (start us, length us, event | category | flops | bytes accessed | tf_op | source)
XLA Modules:
  0.0 326.5 jit_solution(2211187910795424601)
XLA Ops:
  0.6 0.0 copy-start
  0.6 1.6 copy.31
  2.3 2.3 copy.30
  4.6 3.0 pad_maximum_fusion
  7.6 7.9 %stack.2 = bf16[4,256,6144]{2,1,0:T(8,128)(2,1)} broadcast(bf16[256,6144]{1,0:T(8,128)(2,1)} %pad_maximum_fusion), dimensions={1,2} | broadcast | bytes 15728640 | tf_op jit(solution)/shard_map/stack | solution.py:12
  15.5 0.0 copy-start.6
  15.5 0.0 copy-start.2
  15.5 0.0 copy-start.5
  15.5 6.5 %all-to-all-start.2 = ((bf16[4,256,6144]{2,1,0:T(8,128)(2,1)}), bf16[4,256,6144]{2,1,0:T(8,128)(2,1)}, u32[]{:S(2)}, u32[]{:S(2)}) async-start(bf16[4,256,6144]{2,1,0:T(8,128)(2,1)} %stack.2), calls=%async_computation.2 | async-start | bytes 25165824 | tf_op jit(solution)/shard_map/all_to_all | solution.py:13
  22.0 0.0 copy-done.6
  22.0 0.1 copy.25
  22.1 0.1 eq.38
  22.3 0.1 eq.42
  22.4 0.6 reduce-window.6
  23.0 0.2 slice_reduce_fusion
  23.3 0.1 fusion.25
  23.4 0.1 reshape.109
  23.5 0.1 copy.28
  23.6 0.1 copy.29
  23.7 0.1 reshape.110
  23.9 0.0 copy-done.2
  23.9 0.2 fusion.13
  24.1 0.0 copy-done.5
  24.1 0.2 fusion.15
  24.3 0.6 broadcast_in_dim.8
  24.9 1.2 reshape.134
  26.2 4.5 %scatter_custom_fusion = bf16[512,2048]{1,0:T(8,128)(2,1)} fusion(s32[256]{0:T(256)S(1)} %bitcast.82, bf16[256,2048]{1,0:T(8,128)(2,1)} %reshape.134, bf16[]{:T(256)} %constant.45.clone.1), kind=kCustom, calls=%fused_computation.38 | custom fusion | bytes 2097664 | tf_op jit(solution)/shard_map/scatter | solution.py:62
  30.6 130.4 %all-to-all-done.2 = bf16[4,256,6144]{2,1,0:T(8,128)(2,1)} async-done(((bf16[4,256,6144]{2,1,0:T(8,128)(2,1)}), bf16[4,256,6144]{2,1,0:T(8,128)(2,1)}, u32[]{:S(2)}, u32[]{:S(2)}) %all-to-all-start.2) | async-done | bytes 12582944 | tf_op jit(solution)/shard_map/all_to_all | solution.py:13
  161.0 12.2 %all-to-all-start.1 = ((bf16[64,8,2048]{2,1,0:T(8,128)(2,1)}), bf16[64,8,2048]{2,1,0:T(8,128)(2,1)}, u32[]{:S(2)}, u32[]{:S(2)}) async-start(bf16[64,8,2048]{2,1,0:T(8,128)(2,1)} %bitcast.75), calls=%async_computation.1 | async-start | bytes 4194304 | tf_op jit(solution)/shard_map/all_to_all | solution.py:122
  173.2 0.0 copy-start.4
  173.2 1.3 convert_multiply_fusion.2
  174.6 2.5 collective-permute-start
  177.1 0.0 copy-done.4
  177.2 4.8 %collective-permute-done = f32[2,2048]{1,0:T(2,128)S(1)} collective-permute-done((f32[2,2048]{1,0:T(2,128)S(1)}, f32[2,2048]{1,0:T(2,128)S(1)}, u32[]{:S(2)}, u32[]{:S(2)}) %collective-permute-start) | collective-permute-done | bytes 16416 | tf_op jit(solution)/shard_map/ppermute | solution.py:19
  182.0 2.2 fusion.12
  184.2 0.0 copy-start.3
  184.2 4.8 %slice_bitcast_fusion = bf16[1,1024,2048]{2,1,0:T(8,128)(2,1)} fusion(bf16[1024,6144]{1,0:T(8,128)(2,1)} %bitcast.13), kind=kLoop, calls=%fused_computation.2 | loop fusion | bytes 8388608 | tf_op jit(solution)/shard_map/transpose;reshape | solution.py:28
  189.0 35.4 %all-to-all-done.1 = bf16[64,8,2048]{2,1,0:T(8,128)(2,1)} async-done(((bf16[64,8,2048]{2,1,0:T(8,128)(2,1)}), bf16[64,8,2048]{2,1,0:T(8,128)(2,1)}, u32[]{:S(2)}, u32[]{:S(2)}) %all-to-all-start.1) | async-done | bytes 2097184 | tf_op jit(solution)/shard_map/all_to_all | solution.py:122
  224.4 0.0 copy-done.3
  224.4 1.6 broadcast_in_dim.6
  226.0 4.6 %all-to-all-start = ((bf16[4,128,2048]{2,1,0:T(8,128)(2,1)}), bf16[4,128,2048]{2,1,0:T(8,128)(2,1)}, u32[]{:S(2)}, u32[]{:S(2)}) async-start(bf16[4,128,2048]{2,1,0:T(8,128)(2,1)} %broadcast_in_dim.6), calls=%async_computation | async-start | bytes 4194304 | tf_op jit(solution)/shard_map/all_to_all | solution.py:35
  230.6 5.2 %fusion.1 = f32[512,1024]{1,0:T(8,128)S(1)} fusion(bf16[1024,6144]{1,0:T(8,128)(2,1)} %bitcast.13, bf16[64,8,2048]{2,1,0:T(8,128)(2,1)} %all-to-all-done.1), kind=kOutput, calls=%fused_computation.6 | convolution fusion | flops 2147483648 | bytes 8388608 | tf_op jit(solution)/shard_map/dot_general | solution.py:66
  235.8 0.0 copy-start.1
  235.8 5.5 %multiply_convert_fusion = bf16[512,1024]{1,0:T(8,128)(2,1)S(1)} fusion(f32[512,1024]{1,0:T(8,128)S(1)} %fusion.1, bf16[1024,6144]{1,0:T(8,128)(2,1)} %bitcast.13, bf16[64,8,2048]{2,1,0:T(8,128)(2,1)} %all-to-all-done.1), kind=kOutput, calls=%fused_computation.17 | convolution fusion | flops 2150629376 | bytes 9437184 | tf_op jit(solution)/shard_map/dot_general | solution.py:67
  241.3 0.0 copy-done.1
  241.3 0.7 convolution_convert_fusion
  242.1 0.7 convolution_convert_fusion.1
  242.8 0.7 convolution_convert_fusion.2
  243.5 0.7 convolution_convert_fusion.3
  244.2 3.1 fusion.2
  247.4 0.0 copy-start.7
  247.4 8.2 %all-to-all-done = bf16[4,128,2048]{2,1,0:T(8,128)(2,1)} async-done(((bf16[4,128,2048]{2,1,0:T(8,128)(2,1)}), bf16[4,128,2048]{2,1,0:T(8,128)(2,1)}, u32[]{:S(2)}, u32[]{:S(2)}) %all-to-all-start) | async-done | bytes 2097184 | tf_op jit(solution)/shard_map/all_to_all | solution.py:35
  255.6 7.6 %all-to-all-start.3 = ((bf16[64,8,2048]{2,1,0:T(8,128)(2,1)}), bf16[64,8,2048]{2,1,0:T(8,128)(2,1)}, u32[]{:S(2)}, u32[]{:S(2)}) async-start(bf16[64,8,2048]{2,1,0:T(8,128)(2,1)} %fusion.2), calls=%async_computation.3 | async-start | bytes 4194304 | tf_op jit(solution)/shard_map/all_to_all | solution.py:135
  263.2 0.0 copy-done.7
  263.2 0.1 copy.32
  263.3 0.0 copy-done
  263.4 3.6 %convolution_convert_fusion.4 = bf16[512,512]{1,0:T(8,128)(2,1)} fusion(bf16[512,2048]{1,0:T(8,128)(2,1)} %bitcast.3, bf16[2048,512]{1,0:T(8,128)(2,1)S(1)} %copy-done), kind=kOutput, calls=%fused_computation.20 | convolution fusion | flops 1074003968 | bytes 4718592 | tf_op jit(solution)/shard_map/dot_general | solution.py:116
  267.0 47.3 %all-to-all-done.3 = bf16[64,8,2048]{2,1,0:T(8,128)(2,1)} async-done(((bf16[64,8,2048]{2,1,0:T(8,128)(2,1)}), bf16[64,8,2048]{2,1,0:T(8,128)(2,1)}, u32[]{:S(2)}, u32[]{:S(2)}) %all-to-all-start.3) | async-done | bytes 2097184 | tf_op jit(solution)/shard_map/all_to_all | solution.py:135
  314.3 4.2 %gather_fusion = bf16[256,2048]{1,0:T(8,128)(2,1)S(1)} fusion(bf16[512,2048]{1,0:T(8,128)(2,1)} %bitcast.26, s32[1024]{0:T(1024)S(1)} %pad_clamp_fusion), kind=kCustom, calls=%fused_computation | custom fusion | bytes 2098176 | tf_op jit(solution)/shard_map/gather | solution.py:142
  318.5 2.4 reshape.121
  320.9 5.6 %multiply_reduce_fusion = bf16[128,2048]{1,0:T(8,128)(2,1)} fusion(f32[128,2,2048]{2,1,0:T(2,128)} %reshape.121, f32[128,2]{1,0:T(8,128)S(1)} %copy.32), kind=kLoop, calls=%fused_computation.16 | loop fusion | flops 786432 | bytes 2622464 | tf_op jit(solution)/shard_map/reduce_sum | solution.py:146
  (12 shorter events, 0.1 us)
Async XLA Ops:
  0.6 262.7 %copy-start = (bf16[2048,512]{1,0:T(8,128)(2,1)S(1)}, bf16[2048,512]{1,0:T(8,128)(2,1)}, u32[]{:S(2)}) copy-start(bf16[2048,512]{1,0:T(8,128)(2,1)} %param.16) | copy-start | bytes 6291460
  15.5 6.5 %copy-start.6 = (s32[128,2]{0,1:T(2,128)S(1)}, s32[128,2]{0,1:T(2,128)}, u32[]{:S(2)}) copy-start(s32[128,2]{0,1:T(2,128)} %param.22) | copy-start | bytes 3076
  15.5 8.3 %copy-start.2 = (bf16[128,2048]{1,0:T(8,128)(2,1)S(1)}, bf16[128,2048]{1,0:T(8,128)(2,1)}, u32[]{:S(2)}) copy-start(bf16[128,2048]{1,0:T(8,128)(2,1)} %param.17) | copy-start | bytes 1572868
  15.5 8.6 %copy-start.5 = (f32[2048]{0:T(1024)S(1)}, f32[2048]{0:T(1024)}, u32[]{:S(2)}) copy-start(f32[2048]{0:T(1024)} %param.18) | copy-start | bytes 24580
  15.5 145.5 %all-to-all-start.2 = ((bf16[4,256,6144]{2,1,0:T(8,128)(2,1)}), bf16[4,256,6144]{2,1,0:T(8,128)(2,1)}, u32[]{:S(2)}, u32[]{:S(2)}) async-start(bf16[4,256,6144]{2,1,0:T(8,128)(2,1)} %stack.2), calls=%async_computation.2 | async-start | bytes 25165824 | tf_op jit(solution)/shard_map/all_to_all | solution.py:13
  161.0 63.4 %all-to-all-start.1 = ((bf16[64,8,2048]{2,1,0:T(8,128)(2,1)}), bf16[64,8,2048]{2,1,0:T(8,128)(2,1)}, u32[]{:S(2)}, u32[]{:S(2)}) async-start(bf16[64,8,2048]{2,1,0:T(8,128)(2,1)} %bitcast.75), calls=%async_computation.1 | async-start | bytes 4194304 | tf_op jit(solution)/shard_map/all_to_all | solution.py:122
  173.2 3.9 %copy-start.4 = (bf16[3,2048]{1,0:T(4,128)(2,1)S(1)}, bf16[3,2048]{1,0:T(4,128)(2,1)}, u32[]{:S(2)}) copy-start(bf16[3,2048]{1,0:T(4,128)(2,1)} %param.15) | copy-start | bytes 36868
  174.6 7.4 %collective-permute-start = (f32[2,2048]{1,0:T(2,128)S(1)}, f32[2,2048]{1,0:T(2,128)S(1)}, u32[]{:S(2)}, u32[]{:S(2)}) collective-permute-start(f32[2,2048]{1,0:T(2,128)S(1)} %slice.78), channel_id=1, source_target_pairs={{0,1},{1,2},{2,3},{3,4},{4,5},{5,6},{6,7},{7,8},{8,9},{9,10},{10,1... | collective-permute-start | bytes 49160 | tf_op jit(solution)/shard_map/ppermute | solution.py:19
  184.2 40.2 %copy-start.3 = (bf16[128,2048]{1,0:T(8,128)(2,1)S(1)}, bf16[128,2048]{1,0:T(8,128)(2,1)}, u32[]{:S(2)}) copy-start(bf16[128,2048]{1,0:T(8,128)(2,1)} %fusion.12) | copy-start | bytes 1572868
  226.0 29.6 %all-to-all-start = ((bf16[4,128,2048]{2,1,0:T(8,128)(2,1)}), bf16[4,128,2048]{2,1,0:T(8,128)(2,1)}, u32[]{:S(2)}, u32[]{:S(2)}) async-start(bf16[4,128,2048]{2,1,0:T(8,128)(2,1)} %broadcast_in_dim.6), calls=%async_computation | async-start | bytes 4194304 | tf_op jit(solution)/shard_map/all_to_all | solution.py:35
  235.8 5.5 %copy-start.1 = (bf16[1,1024,2048]{2,1,0:T(8,128)(2,1)S(1)}, bf16[1,1024,2048]{2,1,0:T(8,128)(2,1)}, u32[]{:S(2)}) copy-start(bf16[1,1024,2048]{2,1,0:T(8,128)(2,1)} %slice_bitcast_fusion) | copy-start | bytes 12582916
  247.4 15.8 %copy-start.7 = (f32[128,2]{0,1:T(2,128)S(1)}, f32[128,2]{0,1:T(2,128)}, u32[]{:S(2)}) copy-start(f32[128,2]{0,1:T(2,128)} %param.23) | copy-start | bytes 3076
  255.6 58.7 %all-to-all-start.3 = ((bf16[64,8,2048]{2,1,0:T(8,128)(2,1)}), bf16[64,8,2048]{2,1,0:T(8,128)(2,1)}, u32[]{:S(2)}, u32[]{:S(2)}) async-start(bf16[64,8,2048]{2,1,0:T(8,128)(2,1)} %fusion.2), calls=%async_computation.3 | async-start | bytes 4194304 | tf_op jit(solution)/shard_map/all_to_all | solution.py:135
